TPU v7x, 128 devices: a whole 4x4x4 slice. The times are simulated.
128 devices in a mesh: fs: 16 (over z, y), tp: 8 (over x, core).
Axes of the slice: x: 4, y: 4, z: 4, core: 2. Of those that a mesh axis runs over, the one named last changes fastest.
Arguments:
- tokens: bfloat16 [12288, 2048], P('fs', 'tp'), may hold values from -40 to 40
- gain_one: float32 [2048], P('tp'), may hold values from 0.1 to 1.9
- w_gate: float32 [2048, 3072], P('fs', 'tp'), may hold values from -0.125 to 0.125
- w_up: float32 [2048, 3072], P('fs', 'tp'), may hold values from -0.125 to 0.125
- w_down: float32 [3072, 2048], P('tp', 'fs'), may hold values from -0.109375 to 0.109375
- scale_gate: float32 [3072], P('tp'), may hold values from 0.5 to 2
- scale_up: float32 [3072], P('tp'), may hold values from 0.5 to 2
- scale_down: float32 [2048], P('tp'), may hold values from 0.5 to 2
- gain_mix: float32 [2048], P('tp'), may hold values from 0.1 to 1.9
- w_query: float32 [2048, 2048], P('fs', 'tp'), may hold values from -0.125 to 0.125
- w_key: float32 [2048, 2048], P('fs', 'tp'), may hold values from -0.125 to 0.125
- w_value: float32 [2048, 2048], P('fs', 'tp'), may hold values from -0.125 to 0.125
- w_outgate: float32 [2048, 2048], P('fs', 'tp'), may hold values from -0.125 to 0.125
- scale_query: float32 [2048], P('tp'), may hold values from 0.5 to 2
- scale_key: float32 [2048], P('tp'), may hold values from 0.5 to 2
- scale_value: float32 [2048], P('tp'), may hold values from 0.5 to 2
- scale_outgate: float32 [2048], P('tp'), may hold values from 0.5 to 2
- ret_gain: float32 [2048], P('tp'), may hold values from 0.1 to 1.9
- decay_rate: float32 [8], P('tp'), may hold values from 0 to 2
- w_mix: float32 [2048, 2048], P('tp', 'fs'), may hold values from -0.125 to 0.125
- scale_mix: float32 [2048], P('tp'), may hold values from 0.5 to 2
- gain_two: float32 [2048], P('tp'), may hold values from 0.1 to 1.9
Outputs:
- layer_out: bfloat16 [12288, 2048], P('fs', 'tp')
All inputs are finite; a program needn't handle non-finite values.
Results may differ from a plain program's by a relative error of at most 0.022.
Values may be sent and summed in bfloat16 or wider, within the bound.
A program may use at most 128 MiB of HBM per device.

v0:
```python
import jax
import jax.numpy as jnp
from jax import lax
from jax.sharding import PartitionSpec as P

D = 2048
LEN = 256
BLK = 128
EPS = 1e-06
HEAD_EPS = 0.1


def from_everyone(shard, axis):
    copies = jnp.broadcast_to(shard, (lax.axis_size(axis), *shard.shape))
    return lax.all_to_all(copies, axis, split_axis=0, concat_axis=0, tiled=True)


def taken_together(shard, axis):
    return from_everyone(shard, axis).sum(axis=0)


def in_blocks(shard, dim, length):
    shape = shard.shape
    blocks = shard.reshape(*shape[:dim], length, shape[dim] // length, *shape[dim + 1 :])
    return jnp.moveaxis(blocks, dim, 0)


def sent_and_summed(shard, axis, dim):
    length = lax.axis_size(axis)
    blocks = lax.all_to_all(in_blocks(shard, dim, length), axis, 0, 0, tiled=True)
    return jnp.sum(blocks.astype(jnp.float32), axis=0)


def side_by_side(arrays, axis, dim, along):
    widths = [a.shape[along] for a in arrays]
    both = jnp.concatenate(arrays, axis=along)
    out = lax.all_gather(both, axis, axis=dim, tiled=True)
    return tuple(jnp.split(out, [sum(widths[:k]) for k in range(1, len(widths))], axis=along))


def laid_out(blocks, dim):
    blocks = jnp.moveaxis(blocks, 0, dim)
    shape = blocks.shape
    return blocks.reshape(*shape[:dim], shape[dim] * shape[dim + 1], *shape[dim + 2 :])


def gathered_copies(shard, axis, dim):
    return laid_out(from_everyone(shard, axis), dim)


def rotate_pairs(values):
    paired = values.reshape(values.shape[:-1] + (values.shape[-1] // 2, 2))
    return jnp.stack((-paired[..., 1], paired[..., 0]), axis=-1).reshape(values.shape)


def retain(query_rows, key_rows, value_rows, decay_rate, length, block):
    total_rows = query_rows.shape[0]
    heads = decay_rate.shape[0]
    head_size = query_rows.shape[1] // heads
    sequences = total_rows // length
    nblocks = length // block

    def split_heads(values):
        return values.astype(jnp.float32).reshape(sequences, length, heads, head_size)

    freq = 1.0 / 10000.0 ** jnp.linspace(0.0, 1.0, head_size // 2, dtype=jnp.float32)
    freq = jnp.repeat(freq, 2)
    angles = jnp.arange(length, dtype=jnp.float32)[:, None] * freq[None, :]
    sines = jnp.sin(angles)[None, :, None, :]
    cosines = jnp.cos(angles)[None, :, None, :]
    queries = split_heads(query_rows)
    queries = queries * cosines + rotate_pairs(queries) * sines
    keys_all = split_heads(key_rows) * head_size ** (-0.5)
    keys_all = keys_all * cosines + rotate_pairs(keys_all) * sines
    values_all = split_heads(value_rows)
    log_decay = -decay_rate
    offsets = jnp.arange(block, dtype=jnp.float32)
    distance = offsets[:, None] - offsets[None, :]
    inside = jnp.where(
        distance >= 0, jnp.exp(log_decay[:, None, None] * jnp.maximum(distance, 0.0)), 0.0
    )
    query_decay = jnp.exp(log_decay[None, :] * (offsets[:, None] + 1.0))
    key_decay = jnp.exp(log_decay[None, :] * (block - 1.0 - offsets[:, None]))
    block_decay = jnp.exp(log_decay * block)

    def to_blocks(values):
        return jnp.moveaxis(values.reshape(sequences, nblocks, block, heads, head_size), 1, 0)

    def advance(carried, pieces):
        query_blk, key_blk, value_blk = pieces
        scores = jnp.einsum("snhd,smhd->shnm", query_blk, key_blk) * inside
        within = jnp.einsum("shnm,smhe->snhe", scores, value_blk)
        across = jnp.einsum("snhd,shde->snhe", query_blk, carried) * query_decay[None, :, :, None]
        weighted = key_blk * key_decay[None, :, :, None]
        carried = carried * block_decay[None, :, None, None] + jnp.einsum(
            "smhd,smhe->shde", weighted, value_blk
        )
        return (carried, within + across)

    initial = jnp.zeros((sequences, heads, head_size, head_size), jnp.float32)
    _, results = lax.scan(
        advance, initial, (to_blocks(queries), to_blocks(keys_all), to_blocks(values_all))
    )
    results = jnp.moveaxis(results, 0, 1).reshape(sequences, length, heads, head_size)
    results = results * lax.rsqrt(jnp.mean(results * results, axis=-1, keepdims=True) + HEAD_EPS)
    return results.reshape(total_rows, heads * head_size)


def normed_rows(hidden_in, norm_gain):
    widened = hidden_in.astype(jnp.float32)
    totals = taken_together(jnp.sum(widened * widened, axis=1), "tp")
    scaled = widened * lax.rsqrt(totals / D + EPS)[:, None] * norm_gain
    return lax.all_gather(scaled.astype(jnp.bfloat16), "tp", axis=1, tiled=True)


def summed_share(partial_value):
    rounded = lax.optimization_barrier(partial_value.astype(jnp.bfloat16))
    return sent_and_summed(rounded.astype(jnp.float32).astype(jnp.bfloat16), "tp", 1)


def ffn_gathered(features, gate_low, up_low, down_low, scale_gate, scale_up):
    pieces = side_by_side((gate_low, up_low), "fs", 0, 1)
    gate_add = jnp.dot(features, pieces[0], preferred_element_type=jnp.float32)
    up_add = jnp.dot(features, pieces[1], preferred_element_type=jnp.float32)
    hidden = (jax.nn.silu(gate_add * scale_gate) * (up_add * scale_up)).astype(jnp.bfloat16)
    return jnp.dot(hidden, gathered_copies(down_low, "fs", 1), preferred_element_type=jnp.float32)


def per_device(
    tokens,
    gain_one,
    w_gate,
    w_up,
    w_down,
    scale_gate,
    scale_up,
    scale_down,
    gain_mix,
    w_query,
    w_key,
    w_value,
    w_outgate,
    scale_query,
    scale_key,
    scale_value,
    scale_outgate,
    ret_gain,
    decay_rate,
    w_mix,
    scale_mix,
    gain_two,
):
    norm_one, norm_mix, norm_two, down_cols, mix_cols = (
        gain_one,
        gain_mix,
        gain_two,
        scale_down,
        scale_mix,
    )
    gate_low = w_gate.astype(jnp.bfloat16)
    up_low = w_up.astype(jnp.bfloat16)
    down_low = w_down.astype(jnp.bfloat16)
    ffn_one = ffn_gathered(
        normed_rows(tokens, norm_one), gate_low, up_low, down_low, scale_gate, scale_up
    )
    first = (tokens.astype(jnp.float32) + 0.5 * summed_share(ffn_one) * down_cols).astype(
        jnp.bfloat16
    )
    features = normed_rows(first, norm_mix)
    pieces = side_by_side(
        (
            w_query.astype(jnp.bfloat16),
            w_key.astype(jnp.bfloat16),
            w_value.astype(jnp.bfloat16),
            w_outgate.astype(jnp.bfloat16),
        ),
        "fs",
        0,
        1,
    )
    query_pre, key_pre, value_pre, outgate_pre = tuple(
        (jnp.dot(features, piece, preferred_element_type=jnp.float32) for piece in pieces)
    )
    query_rows = (query_pre * scale_query).astype(jnp.bfloat16)
    key_rows = (key_pre * scale_key).astype(jnp.bfloat16)
    value_rows = (value_pre * scale_value).astype(jnp.bfloat16)
    outgate_rows = (outgate_pre * scale_outgate).astype(jnp.bfloat16)
    retained = retain(query_rows, key_rows, value_rows, decay_rate, LEN, BLK)
    mixed = (retained * ret_gain * jax.nn.silu(outgate_rows.astype(jnp.float32))).astype(
        jnp.bfloat16
    )
    mix_partial = jnp.dot(
        mixed,
        gathered_copies(w_mix.astype(jnp.bfloat16), "fs", 1),
        preferred_element_type=jnp.float32,
    )
    second = (first.astype(jnp.float32) + summed_share(mix_partial) * mix_cols).astype(jnp.bfloat16)
    ffn_two = ffn_gathered(
        normed_rows(second, norm_two), gate_low, up_low, down_low, scale_gate, scale_up
    )
    result = (second.astype(jnp.float32) + 0.5 * summed_share(ffn_two) * down_cols).astype(
        jnp.bfloat16
    )
    return result


def solution(mesh):
    return jax.shard_map(
        per_device,
        mesh=mesh,
        in_specs=(
            P("fs", "tp"),
            P("tp"),
            P("fs", "tp"),
            P("fs", "tp"),
            P("tp", "fs"),
            P("tp"),
            P("tp"),
            P("tp"),
            P("tp"),
            P("fs", "tp"),
            P("fs", "tp"),
            P("fs", "tp"),
            P("fs", "tp"),
            P("tp"),
            P("tp"),
            P("tp"),
            P("tp"),
            P("tp"),
            P("tp"),
            P("tp", "fs"),
            P("tp"),
            P("tp"),
        ),
        out_specs=P("fs", "tp"),
        check_vma=False,
    )
```

profile of v0, /device:TPU:1, one launch (start us, length us, event | category | flops | bytes accessed | tf_op | source)
XLA Modules:
  0.0 379.9 jit_solution(7782225091500418627)
XLA Ops:
  7.9 10.3 %all_to_all.44 = f32[8,1,768]{2,1,0:T(1,128)S(1)} all-to-all(f32[8,1,768]{2,1,0:T(1,128)S(1)} %broadcast_in_dim.23), channel_id=1, replica_groups=mesh['fs'=16,'tp'=8] {'tp'}, dimensions={0} | all-to-all | bytes 49152 | tf_op jit(solution)/shard_map/all_to_all | solution.py:15
  26.1 7.8 %all-to-all-start.1 = ((bf16[16,384,128]{1,2,0:T(8,128)(2,1)}), bf16[16,384,128]{1,2,0:T(8,128)(2,1)S(1)}, u32[]{:S(2)}, u32[]{:S(2)}) async-start(bf16[16,384,128]{1,2,0:T(8,128)(2,1)} %broadcast_in_dim.24), calls=%async_computation.1 | async-start | bytes 3145728 | tf_op jit(solution)/shard_map/all_to_all | solution.py:15
  33.9 18.4 %all-gather.6.cloned.1.call-done = bf16[768,2048]{1,0:T(8,128)(2,1)} async-done(((bf16[768,256]{1,0:T(8,128)(2,1)}), bf16[768,2048]{1,0:T(8,128)(2,1)}) %all-gather.6.cloned.1.call-update) | async-done | bytes 3145744 | tf_op jit(solution)/shard_map/all_gather | solution.py:113
  52.3 50.1 %all-gather.8.cloned.1.call-done = bf16[2048,768]{1,0:T(8,128)(2,1)} async-done(((bf16[128,768]{1,0:T(8,128)(2,1)}), bf16[2048,768]{1,0:T(8,128)(2,1)}) %all-gather.8.cloned.1.call-update) | async-done | bytes 3145744 | tf_op jit(solution)/shard_map/all_gather | solution.py:37
  102.4 5.2 %convolution_multiply_fusion.4 = f32[768,384]{1,0:T(8,128)} fusion(bf16[768,2048]{1,0:T(8,128)(2,1)} %all-gather.6.cloned.1.call-done, bf16[2048,768]{1,0:T(8,128)(2,1)} %all-gather.8.cloned.1.call-done, f32[384]{0:T(512)S(1)} %copy-done.21), kind=kOutput, calls=%fused_computation.47 | convolution fusion | flops 1208254464 | bytes 5899776 | tf_op jit(solution)/shard_map/dot_general | solution.py:123
  108.8 6.7 %convolution_convert_fusion.2 = bf16[768,2048]{1,0:T(8,128)(2,1)S(1)} fusion(bf16[384,2048]{0,1:T(8,128)(2,1)} %bitcast.163, bf16[768,2048]{1,0:T(8,128)(2,1)} %all-gather.6.cloned.1.call-done, bf16[2048,768]{1,0:T(8,128)(2,1)} %all-gather.8.cloned.1.call-done, f32[768,384]{1,0:T(8,128)} %convolution_multiply_fusion.4, f32[384]{0:T(512)S(1)} %copy-done.22), kind=kOutput, calls=%fused_computation.38 | convolution fusion | flops 2419556352 | bytes 10618368 | tf_op jit(solution)/shard_map/dot_general | solution.py:126
  117.4 5.7 %all-to-all-start.2 = ((bf16[8,768,256]{2,1,0:T(8,128)(2,1)}), bf16[8,768,256]{2,1,0:T(8,128)(2,1)S(1)}, u32[]{:S(2)}, u32[]{:S(2)}) async-start(bf16[8,768,256]{2,1,0:T(8,128)(2,1)} %bitcast.116), calls=%async_computation.2 | async-start | bytes 6291456 | tf_op jit(solution)/shard_map/all_to_all | solution.py:30
  123.1 37.4 %all-to-all-done.2 = bf16[8,768,256]{2,1,0:T(8,128)(2,1)S(1)} async-done(((bf16[8,768,256]{2,1,0:T(8,128)(2,1)}), bf16[8,768,256]{2,1,0:T(8,128)(2,1)S(1)}, u32[]{:S(2)}, u32[]{:S(2)}) %all-to-all-start.2) | async-done | bytes 3145760 | tf_op jit(solution)/shard_map/all_to_all | solution.py:30
  161.2 8.0 %all_to_all.45 = f32[8,1,768]{2,1,0:T(1,128)S(1)} all-to-all(f32[8,1,768]{2,1,0:T(1,128)S(1)} %broadcast_in_dim.27), channel_id=1, replica_groups=mesh['fs'=16,'tp'=8] {'tp'}, dimensions={0} | all-to-all | bytes 49152 | tf_op jit(solution)/shard_map/all_to_all | solution.py:15
  172.3 4.3 %all-to-all-start.4 = ((bf16[16,256,128]{1,2,0:T(8,128)(2,1)}), bf16[16,256,128]{1,2,0:T(8,128)(2,1)}, u32[]{:S(2)}, u32[]{:S(2)}) async-start(bf16[16,256,128]{1,2,0:T(8,128)(2,1)} %broadcast_in_dim.31), calls=%async_computation.4 | async-start | bytes 2097152 | tf_op jit(solution)/shard_map/all_to_all | solution.py:15
  178.0 8.5 %multiply_cosine_fusion = (f32[2,128,256]{1,0,2:T(2,128)}, f32[2,128,256]{1,0,2:T(2,128)}, f32[2,128,256]{1,0,2:T(2,128)}) fusion(f32[2,128]{1,0:T(2,128)S(1)} %multiply_add_fusion, f32[256]{0:T(256)S(1)} %mul.470), kind=kLoop, calls=%fused_computation.107 | loop fusion | flops 327680 | bytes 788480 | tf_op jit(solution)/shard_map/cos | solution.py:70
  186.5 12.2 %all-gather.10.cloned.1.call-done = bf16[768,2048]{1,0:T(8,128)(2,1)} async-done(((bf16[768,256]{1,0:T(8,128)(2,1)}), bf16[768,2048]{1,0:T(8,128)(2,1)}) %all-gather.10.cloned.1.call-update) | async-done | bytes 3145744 | tf_op jit(solution)/shard_map/all_gather | solution.py:113
  198.7 4.1 %broadcast_multiply_fusion = (f32[768,256]{1,0:T(8,128)S(1)}, f32[768,256]{1,0:T(8,128)}) fusion(f32[256]{0:T(256)S(1)} %copy-done.24, bf16[768,2048]{1,0:T(8,128)(2,1)} %all-gather.10.cloned.1.call-done, bf16[2048,1024]{1,0:T(8,128)(2,1)} %all-gather.12.cloned.1.call-done), kind=kOutput, calls=%fused_computation.106 | convolution fusion | flops 806092800 | bytes 5768192 | tf_op jit(solution)/shard_map/dot_general | solution.py:182
  205.7 2.2 fusion.41
  213.3 3.3 fusion.39
  218.5 8.8 %while.15 = (s32[]{:T(128)}, f32[3,1,256,256]{3,2,0,1:T(8,128)S(1)}, f32[2,3,128,1,256]{2,4,1,3,0:T(8,128)}, f32[1]{0:T(128)}, f32[2,3,128,1,256]{2,0,3,4,1:T(2,...) while((s32[]{:T(128)}, ...), condition=%wide.region_6.7_spmd.clone.clone.clone, body=%wide.region_5.6_spmd.clone.clone.clone.sunk | while | flops 152257024 | bytes 7998088 | solution.py:101
  230.0 3.2 fusion.66
  233.3 2.2 convolution_convert_fusion.1
  235.7 41.4 %all_to_all.46 = bf16[8,768,256]{2,1,0:T(8,128)(2,1)S(1)} all-to-all(bf16[8,768,256]{2,1,0:T(8,128)(2,1)S(1)} %bitcast.155), channel_id=1, replica_groups=mesh['fs'=16,'tp'=8] {'tp'}, dimensions={0} | all-to-all | bytes 6291456 | tf_op jit(solution)/shard_map/all_to_all | solution.py:30
  278.4 8.1 %all_to_all.47 = f32[8,1,768]{2,1,0:T(1,128)S(1)} all-to-all(f32[8,1,768]{2,1,0:T(1,128)S(1)} %broadcast_in_dim.32), channel_id=1, replica_groups=mesh['fs'=16,'tp'=8] {'tp'}, dimensions={0} | all-to-all | bytes 49152 | tf_op jit(solution)/shard_map/all_to_all | solution.py:15
  287.5 31.1 %all-gather.14.cloned.1.call-done = bf16[768,2048]{1,0:T(8,128)(2,1)} async-done(((bf16[768,256]{1,0:T(8,128)(2,1)}), bf16[768,2048]{1,0:T(8,128)(2,1)}) %all-gather.14.cloned.1.call-update) | async-done | bytes 3145744 | tf_op jit(solution)/shard_map/all_gather | solution.py:113
  318.6 5.3 %convolution_multiply_fusion.2 = f32[768,384]{1,0:T(8,128)} fusion(bf16[768,2048]{1,0:T(8,128)(2,1)} %all-gather.14.cloned.1.call-done, bf16[2048,768]{1,0:T(8,128)(2,1)} %all-gather.8.cloned.1.call-done, f32[384]{0:T(512)S(1)} %copy-done.21), kind=kOutput, calls=%fused_computation.44 | convolution fusion | flops 1208254464 | bytes 5899776 | tf_op jit(solution)/shard_map/dot_general | solution.py:123
  323.8 6.6 %convolution_convert_fusion = bf16[768,2048]{1,0:T(8,128)(2,1)S(1)} fusion(bf16[384,2048]{0,1:T(8,128)(2,1)} %bitcast.164, bf16[768,2048]{1,0:T(8,128)(2,1)} %all-gather.14.cloned.1.call-done, bf16[2048,768]{1,0:T(8,128)(2,1)} %all-gather.8.cloned.1.call-done, f32[768,384]{1,0:T(8,128)} %convolution_multiply_fusion.2, f32[384]{0:T(512)S(1)} %copy-done.23), kind=kOutput, calls=%fused_computation.36 | convolution fusion | flops 2419556352 | bytes 10618368 | tf_op jit(solution)/shard_map/dot_general | solution.py:126
  330.7 41.4 %all_to_all.48 = bf16[8,768,256]{2,1,0:T(8,128)(2,1)S(1)} all-to-all(bf16[8,768,256]{2,1,0:T(8,128)(2,1)S(1)} %bitcast.156), channel_id=1, replica_groups=mesh['fs'=16,'tp'=8] {'tp'}, dimensions={0} | all-to-all | bytes 6291456 | tf_op jit(solution)/shard_map/all_to_all | solution.py:30
  (148 shorter events, 41.6 us)
Async XLA Ops:
  6.5 17.2 %copy-start.13 = (f32[128,256]{1,0:T(8,128)S(1)}, f32[128,256]{1,0:T(8,128)}, u32[]{:S(2)}) copy-start(f32[128,256]{1,0:T(8,128)} %param.34) | copy-start | bytes 393220
  6.5 17.2 %copy-start.14 = (f32[128,256]{1,0:T(8,128)S(1)}, f32[128,256]{1,0:T(8,128)}, u32[]{:S(2)}) copy-start(f32[128,256]{1,0:T(8,128)} %param.35) | copy-start | bytes 393220
  6.5 17.3 %copy-start.15 = (f32[128,256]{1,0:T(8,128)S(1)}, f32[128,256]{1,0:T(8,128)}, u32[]{:S(2)}) copy-start(f32[128,256]{1,0:T(8,128)} %param.36) | copy-start | bytes 393220
  6.5 18.1 %copy-start.12 = (f32[384,128]{1,0:T(8,128)S(1)}, f32[384,128]{1,0:T(8,128)}, u32[]{:S(2)}) copy-start(f32[384,128]{1,0:T(8,128)} %param.28) | copy-start | bytes 589828
  6.5 45.8 %all-gather.6.cloned.1.call-start = ((), (), s32[]{:S(2)}) async-start(), calls=%async_computation.8 | async-start | bytes 3538944 | tf_op jit(solution)/shard_map/all_gather | solution.py:113
  20.1 82.3 %all-gather.8.cloned.1.call-start = ((), (), s32[]{:S(2)}) async-start(), calls=%async_computation.9 | async-start | bytes 3342336 | tf_op jit(solution)/shard_map/all_gather | solution.py:37
  22.8 163.7 %all-gather.12.cloned.1.call-start = ((), (), s32[]{:S(2)}) async-start(), calls=%async_computation.11 | async-start | bytes 4456448 | tf_op jit(solution)/shard_map/all_gather | solution.py:37
  23.8 78.6 %copy-start.21 = (f32[384]{0:T(512)S(1)}, f32[384]{0:T(512)}, u32[]{:S(2)}) copy-start(f32[384]{0:T(512)} %param.29) | copy-start | bytes 4612
  26.1 81.5 %all-to-all-start.1 = ((bf16[16,384,128]{1,2,0:T(8,128)(2,1)}), bf16[16,384,128]{1,2,0:T(8,128)(2,1)S(1)}, u32[]{:S(2)}, u32[]{:S(2)}) async-start(bf16[16,384,128]{1,2,0:T(8,128)(2,1)} %broadcast_in_dim.24), calls=%async_computation.1 | async-start | bytes 3145728 | tf_op jit(solution)/shard_map/all_to_all | solution.py:15
  33.9 74.9 %copy-start.22 = (f32[384]{0:T(512)S(1)}, f32[384]{0:T(512)}, u32[]{:S(2)}) copy-start(f32[384]{0:T(512)} %param.30) | copy-start | bytes 4612
  117.4 5.7 %copy-start.18 = (f32[256]{0:T(256)S(1)}, f32[256]{0:T(256)}, u32[]{:S(2)}) copy-start(f32[256]{0:T(256)} %param.31) | copy-start | bytes 3076
  117.4 43.1 %all-to-all-start.2 = ((bf16[8,768,256]{2,1,0:T(8,128)(2,1)}), bf16[8,768,256]{2,1,0:T(8,128)(2,1)S(1)}, u32[]{:S(2)}, u32[]{:S(2)}) async-start(bf16[8,768,256]{2,1,0:T(8,128)(2,1)} %bitcast.116), calls=%async_computation.2 | async-start | bytes 6291456 | tf_op jit(solution)/shard_map/all_to_all | solution.py:30
  123.1 37.9 %copy-start = (bf16[768,256]{1,0:T(8,128)(2,1)S(1)}, bf16[768,256]{1,0:T(8,128)(2,1)}, u32[]{:S(2)}) copy-start(bf16[768,256]{1,0:T(8,128)(2,1)} %param.24) | copy-start | bytes 1179652
  123.1 46.2 %copy-start.16 = (f32[256]{0:T(256)S(1)}, f32[256]{0:T(256)}, u32[]{:S(2)}) copy-start(f32[256]{0:T(256)} %param.32) | copy-start | bytes 3076
  123.1 75.6 %all-gather.10.cloned.1.call-start = ((), (), s32[]{:S(2)}) async-start(), calls=%async_computation.10 | async-start | bytes 3538944 | tf_op jit(solution)/shard_map/all_gather | solution.py:113
  161.2 15.5 %copy-start.1 = (bf16[768,256]{1,0:T(8,128)(2,1)}, bf16[768,256]{1,0:T(8,128)(2,1)S(1)}, u32[]{:S(2)}) copy-start(bf16[768,256]{1,0:T(8,128)(2,1)S(1)} %get-tuple-element.210) | copy-start | bytes 1179652
  161.2 37.5 %copy-start.24 = (f32[256]{0:T(256)S(1)}, f32[256]{0:T(256)}, u32[]{:S(2)}) copy-start(f32[256]{0:T(256)} %param.38) | copy-start | bytes 3076
  172.3 60.9 %all-to-all-start.4 = ((bf16[16,256,128]{1,2,0:T(8,128)(2,1)}), bf16[16,256,128]{1,2,0:T(8,128)(2,1)}, u32[]{:S(2)}, u32[]{:S(2)}) async-start(bf16[16,256,128]{1,2,0:T(8,128)(2,1)} %broadcast_in_dim.31), calls=%async_computation.4 | async-start | bytes 2097152 | tf_op jit(solution)/shard_map/all_to_all | solution.py:15
  176.7 141.9 %all-gather.14.cloned.1.call-start = ((), (), s32[]{:S(2)}) async-start(), calls=%async_computation.12 | async-start | bytes 3538944 | tf_op jit(solution)/shard_map/all_gather | solution.py:113
  208.9 4.3 %copy-start.26 = (f32[256]{0:T(256)S(1)}, f32[256]{0:T(256)}, u32[]{:S(2)}) copy-start(f32[256]{0:T(256)} %param.39) | copy-start | bytes 3076
  218.5 11.5 %copy-start.27 = (f32[256]{0:T(256)S(1)}, f32[256]{0:T(256)}, u32[]{:S(2)}) copy-start(f32[256]{0:T(256)} %param.40) | copy-start | bytes 3076
  218.5 11.5 %copy-start.28 = (f32[256]{0:T(256)S(1)}, f32[256]{0:T(256)}, u32[]{:S(2)}) copy-start(f32[256]{0:T(256)} %param.41) | copy-start | bytes 3076
  277.1 9.4 %copy-start.17 = (f32[256]{0:T(256)S(1)}, f32[256]{0:T(256)}, u32[]{:S(2)}) copy-start(f32[256]{0:T(256)} %param.45) | copy-start | bytes 3076
  287.4 36.4 %copy-start.23 = (f32[384]{0:T(512)S(1)}, f32[384]{0:T(512)}, u32[]{:S(2)}) copy-start(f32[384]{0:T(512)} %param.30) | copy-start | bytes 4612
  (13 other events, 33.6 us)
Sparse Core Ops, SparseCore 0:
  20.2 32.0 all-gather.5
  54.5 47.8 all-gather.7
  104.5 50.5 all-gather.11
  170.3 28.3 all-gather.9
  287.6 30.9 all-gather.13
where the time goes:
time: 381 us; the launch traced here: 380 us
  waiting for transfers between devices  149 us (39%)
  blocking collectives  109 us (29%)
  matrix products  42.7 us (11%)
  other arithmetic  25.7 us (7%)
  local copies, waits for them, and re-layouts  20.2 us (5%)
  starting transfers between devices  18.2 us (5%)
  between operations  14.5 us (4%)
    all_to_all x2, blocking collectives, sent_and_summed(): lax.all_to_all(in_blocks(shard, dim, length), axis, 0, 0, tiled=True)  82.8 us
    all_gather x3, waiting for transfers between devices, normed_rows(): return lax.all_gather(scaled.astype(jnp.bfloat16), 'tp', axis=1, tiled=True)  61.7 us
    all_gather x2, waiting for transfers between devices, side_by_side(): out = lax.all_gather(both, axis, axis=dim, tiled=True)  50.1 us
    all_to_all x1, waiting for transfers between devices, sent_and_summed(): lax.all_to_all(in_blocks(shard, dim, length), axis, 0, 0, tiled=True)  37.4 us
    all_to_all x3, blocking collectives, from_everyone(): return lax.all_to_all(copies, axis, split_axis=0, concat_axis=0, tiled=True)  26.4 us
    dot_general x2, matrix products, ffn_gathered(): jnp.dot(hidden, gathered_copies(down_low, 'fs', 1), preferred_element_typ...  13.3 us
    dot_general x4, matrix products, per_device(): jnp.dot(features, piece, preferred_element_type=jnp.float32)  12.8 us
    all_to_all x2, starting transfers between devices, from_everyone(): return lax.all_to_all(copies, axis, split_axis=0, concat_axis=0, tiled=True)  12.1 us
  transfers between devices with their start and end apart: 8, of which 5 were waited for; matrix products, arithmetic and copies ran while one was open for 17% of the time, Pallas kernels for 0%

commit v1 on v0

--- a/solution.py
+++ b/solution.py
@@ -8,6 +8,28 @@
 BLK = 128
 EPS = 1e-06
 HEAD_EPS = 0.1
+
+
+def joined_along(blocks, dim):
+    shape = list(blocks.shape[1:])
+    shape[dim] *= blocks.shape[0]
+    return jnp.moveaxis(blocks, 0, dim).reshape(shape)
+
+
+def collect(value, axis, dim):
+    devices = lax.axis_size(axis)
+    pairs = [(i, (i + 1) % devices) for i in range(devices)]
+    back = [(b, a) for a, b in pairs]
+    lower, upper = ([], [])
+    for hop in range(devices - 1):
+        if hop % 2 == 0:
+            lower.append(lax.ppermute(lower[-1] if lower else value, axis, pairs))
+        else:
+            upper.append(lax.ppermute(upper[-1] if upper else value, axis, back))
+    parts = jnp.stack([*lower[::-1], value, *upper])
+    shift = lax.axis_index(axis) - len(lower)
+    parts = parts[(jnp.arange(devices) - shift) % devices]
+    return joined_along(parts, dim)
 
 
 def from_everyone(shard, axis):
@@ -110,7 +132,7 @@
     widened = hidden_in.astype(jnp.float32)
     totals = taken_together(jnp.sum(widened * widened, axis=1), "tp")
     scaled = widened * lax.rsqrt(totals / D + EPS)[:, None] * norm_gain
-    return lax.all_gather(scaled.astype(jnp.bfloat16), "tp", axis=1, tiled=True)
+    return collect(scaled.astype(jnp.bfloat16), "tp", 1)
 
 
 def summed_share(partial_value):

time: 381 us -> 403 us (1.058)
  waiting for transfers between devices: 149 us -> 70 us
  starting transfers between devices: 18.2 us -> 64.8 us
  local copies, waits for them, and re-layouts: 20.2 us -> 62.4 us
  blocking collectives: 109 us -> 118 us
    all_gather x3 -> x0, waiting for transfers between devices: 61.7 us -> none  [normed_rows(): return lax.all_gather(scaled.astype(jnp.bfloat16), 'tp', axis=1, tiled=True)]
    all_gather x2, waiting for transfers between devices: 50.1 us -> 0.01 us  [side_by_side(): out = lax.all_gather(both, axis, axis=dim, tiled=True)]
    ppermute x0 -> x21, starting transfers between devices: none -> 41.5 us  [the longest x12 22.6 us: collect(): lower.append(lax.ppermute(lower[-1] if lower else value, axis, pairs))]
    ppermute x0 -> x21, waiting for transfers between devices: none -> 32.6 us  [the longest x12 31.4 us: collect(): lower.append(lax.ppermute(lower[-1] if lower else value, axis, pairs))]
    unnamed x58 -> x82, local copies, waits for them, and re-layouts: 1.8 us -> 15 us
    transpose x0 -> x3, local copies, waits for them, and re-layouts: none -> 10.5 us  [joined_along(): return jnp.moveaxis(blocks, 0, dim).reshape(shape)]
    gather x0 -> x3, local copies, waits for them, and re-layouts: none -> 9.65 us  [collect(): parts = parts[(jnp.arange(devices) - shift) % devices]]
    all_to_all x2, blocking collectives: 82.8 us -> 91.1 us  [sent_and_summed(): lax.all_to_all(in_blocks(shard, dim, length), axis, 0, 0, tiled=True)]
  transfers between devices with their start and end apart: 8 -> 26, of which waited for: 5 -> 13; matrix products, arithmetic and copies ran while one was open for 17% -> 26% of each run, Pallas kernels for 0% -> 0%
where the time goes in v1:
time: 403 us; the launch traced here: 402 us
  blocking collectives  118 us (29%)
  waiting for transfers between devices  70 us (17%)
  starting transfers between devices  64.8 us (16%)
  local copies, waits for them, and re-layouts  62.4 us (15%)
  matrix products  44.7 us (11%)
  other arithmetic  27.4 us (7%)
  between operations  14.8 us (4%)
    all_to_all x2, blocking collectives, sent_and_summed(): lax.all_to_all(in_blocks(shard, dim, length), axis, 0, 0, tiled=True)  91.1 us
    all_to_all x1, waiting for transfers between devices, sent_and_summed(): lax.all_to_all(in_blocks(shard, dim, length), axis, 0, 0, tiled=True)  37.4 us
    ppermute x12, waiting for transfers between devices, collect(): lower.append(lax.ppermute(lower[-1] if lower else value, axis, pairs))  31.4 us
    all_to_all x3, blocking collectives, from_everyone(): return lax.all_to_all(copies, axis, split_axis=0, concat_axis=0, tiled=True)  26.5 us
    ppermute x12, starting transfers between devices, collect(): lower.append(lax.ppermute(lower[-1] if lower else value, axis, pairs))  22.6 us
    ppermute x9, starting transfers between devices, collect(): upper.append(lax.ppermute(upper[-1] if upper else value, axis, back))  18.9 us
    unnamed x82, local copies, waits for them, and re-layouts  15 us
    dot_general x2, matrix products, ffn_gathered(): jnp.dot(hidden, gathered_copies(down_low, 'fs', 1), preferred_element_typ...  14.8 us
  transfers between devices with their start and end apart: 26, of which 13 were waited for; matrix products, arithmetic and copies ran while one was open for 26% of the time, Pallas kernels for 0%

profile of v1, /device:TPU:1, one launch (start us, length us, event | category | flops | bytes accessed | tf_op | source)
XLA Modules:
  0.0 401.8 jit_solution(2769023523494886376)
XLA Ops:
  10.4 10.4 %all_to_all.44 = f32[8,1,768]{2,1,0:T(1,128)S(1)} all-to-all(f32[8,1,768]{2,1,0:T(1,128)S(1)} %broadcast_in_dim.23), channel_id=1, replica_groups=mesh['fs'=16,'tp'=8] {'tp'}, dimensions={0} | all-to-all | bytes 49152 | tf_op jit(solution)/shard_map/all_to_all | solution.py:37
  23.0 4.7 %collective-permute-done = bf16[768,256]{1,0:T(8,128)(2,1)S(1)} collective-permute-done((bf16[768,256]{1,0:T(8,128)(2,1)S(1)}, bf16[768,256]{1,0:T(8,128)(2,1)S(1)}, u32[]{:S(2)}, u32[]{:S(2)}) %collective-permute-start) | collective-permute-done | bytes 393248 | tf_op jit(solution)/shard_map/ppermute | solution.py:26
  47.0 7.8 %all-to-all-start.1 = ((bf16[16,384,128]{1,2,0:T(8,128)(2,1)}), bf16[16,384,128]{1,2,0:T(8,128)(2,1)}, u32[]{:S(2)}, u32[]{:S(2)}) async-start(bf16[16,384,128]{1,2,0:T(8,128)(2,1)} %broadcast_in_dim.24), calls=%async_computation.1 | async-start | bytes 3145728 | tf_op jit(solution)/shard_map/all_to_all | solution.py:37
  55.9 3.8 collective-permute-start.6
  71.7 5.4 %convolution_multiply_fusion.4 = f32[768,384]{1,0:T(8,128)} fusion(bf16[768,2048]{0,1:T(8,128)(2,1)} %bitcast.220, bf16[2048,768]{1,0:T(8,128)(2,1)} %all-gather.3.cloned.1.call-done, f32[384]{0:T(512)S(1)} %copy-done.23), kind=kOutput, calls=%fused_computation.50 | convolution fusion | flops 1208254464 | bytes 5899776 | tf_op jit(solution)/shard_map/dot_general | solution.py:145
  77.1 7.5 %convolution_convert_fusion.2 = bf16[768,2048]{1,0:T(8,128)(2,1)} fusion(bf16[384,2048]{0,1:T(8,128)(2,1)} %bitcast.12, bf16[768,2048]{0,1:T(8,128)(2,1)S(1)} %bitcast.221, bf16[2048,768]{1,0:T(8,128)(2,1)} %all-gather.3.cloned.1.call-done, f32[768,384]{1,0:T(8,128)} %convolution_multiply_fusion.4, f32[384]{0:T(512)S(1)} %copy-done.25), kind=kOutput, calls=%fused_computation.41 | convolution fusion | flops 2419556352 | bytes 10618368 | tf_op jit(solution)/shard_map/dot_general | solution.py:148
  84.6 3.9 copy.171
  88.5 10.9 %all-to-all-start.2 = ((bf16[8,768,256]{2,1,0:T(8,128)(2,1)}), bf16[8,768,256]{2,1,0:T(8,128)(2,1)S(1)}, u32[]{:S(2)}, u32[]{:S(2)}) async-start(bf16[8,768,256]{2,1,0:T(8,128)(2,1)} %bitcast.172), calls=%async_computation.2 | async-start | bytes 6291456 | tf_op jit(solution)/shard_map/all_to_all | solution.py:52
  99.4 37.4 %all-to-all-done.2 = bf16[8,768,256]{2,1,0:T(8,128)(2,1)S(1)} async-done(((bf16[8,768,256]{2,1,0:T(8,128)(2,1)}), bf16[8,768,256]{2,1,0:T(8,128)(2,1)S(1)}, u32[]{:S(2)}, u32[]{:S(2)}) %all-to-all-start.2) | async-done | bytes 3145760 | tf_op jit(solution)/shard_map/all_to_all | solution.py:52
  137.5 8.0 %all_to_all.45 = f32[8,1,768]{2,1,0:T(1,128)S(1)} all-to-all(f32[8,1,768]{2,1,0:T(1,128)S(1)} %broadcast_in_dim.27), channel_id=1, replica_groups=mesh['fs'=16,'tp'=8] {'tp'}, dimensions={0} | all-to-all | bytes 49152 | tf_op jit(solution)/shard_map/all_to_all | solution.py:37
  146.7 4.7 %collective-permute-done.7 = bf16[768,256]{1,0:T(8,128)(2,1)S(1)} collective-permute-done((bf16[768,256]{1,0:T(8,128)(2,1)S(1)}, bf16[768,256]{1,0:T(8,128)(2,1)S(1)}, u32[]{:S(2)}, u32[]{:S(2)}) %collective-permute-start.7) | collective-permute-done | bytes 393248 | tf_op jit(solution)/shard_map/ppermute | solution.py:26
  154.9 3.7 collective-permute-done.8
  163.2 4.5 %all-to-all-start.4 = ((bf16[16,256,128]{1,2,0:T(8,128)(2,1)}), bf16[16,256,128]{1,2,0:T(8,128)(2,1)}, u32[]{:S(2)}, u32[]{:S(2)}) async-start(bf16[16,256,128]{1,2,0:T(8,128)(2,1)} %broadcast_in_dim.29), calls=%async_computation.4 | async-start | bytes 2097152 | tf_op jit(solution)/shard_map/all_to_all | solution.py:37
  174.3 9.2 %multiply_cosine_fusion = (f32[2,128,256]{1,0,2:T(2,128)}, f32[2,128,256]{1,0,2:T(2,128)}, f32[2,128,256]{1,0,2:T(2,128)}) fusion(f32[2,128]{1,0:T(2,128)S(1)} %multiply_add_fusion, f32[256]{0:T(256)} %mul.470), kind=kLoop, calls=%fused_computation.134 | loop fusion | flops 327680 | bytes 788480 | tf_op jit(solution)/shard_map/cos | solution.py:92
  193.0 4.4 %gather_fusion.1 = bf16[8,768,256]{2,1,0:T(8,128)(2,1)} fusion(bf16[8,768,256]{2,1,0:T(8,128)(2,1)} %bitcast_dynamic-update-slice_fusion.8, s32[1024]{0:T(1024)S(1)} %pad_clamp_fusion), kind=kCustom, calls=%fused_computation.1 | custom fusion | bytes 6291488 | tf_op jit(solution)/shard_map/gather | solution.py:31
  197.4 4.8 %copy.135 = bf16[768,8,256]{0,2,1:T(8,128)(2,1)} copy(bf16[768,8,256]{2,0,1:T(8,128)(2,1)} %bitcast.213) | data formatting | bytes 6291456 | tf_op jit(solution)/shard_map/transpose | solution.py:16
  202.2 4.2 %broadcast_multiply_fusion = (f32[768,256]{1,0:T(8,128)S(1)}, f32[768,256]{1,0:T(8,128)}) fusion(f32[256]{0:T(256)S(1)} %copy-done.27, bf16[768,2048]{0,1:T(8,128)(2,1)} %bitcast.216, bf16[2048,1024]{1,0:T(8,128)(2,1)} %all-gather.5.cloned.1.call-done), kind=kOutput, calls=%fused_computation.133 | convolution fusion | flops 806092800 | bytes 5768192 | tf_op jit(solution)/shard_map/dot_general | solution.py:204
  222.0 8.6 %while.15 = (s32[]{:T(128)}, f32[3,1,256,256]{3,2,0,1:T(8,128)S(1)}, f32[2,3,128,1,256]{2,4,1,3,0:T(8,128)}, f32[1]{0:T(128)}, f32[2,3,128,1,256]{2,0,3,4,1:T(2,...) while((s32[]{:T(128)}, ...), condition=%wide.region_6.7_spmd.clone.clone.clone, body=%wide.region_5.6_spmd.clone.clone.clone.sunk | while | flops 152257024 | bytes 7998088 | solution.py:123
  239.1 44.1 %all_to_all.46 = bf16[8,768,256]{2,1,0:T(8,128)(2,1)S(1)} all-to-all(bf16[8,768,256]{2,1,0:T(8,128)(2,1)S(1)} %bitcast.214), channel_id=1, replica_groups=mesh['fs'=16,'tp'=8] {'tp'}, dimensions={0} | all-to-all | bytes 6291456 | tf_op jit(solution)/shard_map/all_to_all | solution.py:52
  284.4 8.1 %all_to_all.47 = f32[8,1,768]{2,1,0:T(1,128)S(1)} all-to-all(f32[8,1,768]{2,1,0:T(1,128)S(1)} %broadcast_in_dim.32), channel_id=1, replica_groups=mesh['fs'=16,'tp'=8] {'tp'}, dimensions={0} | all-to-all | bytes 49152 | tf_op jit(solution)/shard_map/all_to_all | solution.py:37
  293.6 4.7 %collective-permute-done.14 = bf16[768,256]{1,0:T(8,128)(2,1)S(1)} collective-permute-done((bf16[768,256]{1,0:T(8,128)(2,1)S(1)}, bf16[768,256]{1,0:T(8,128)(2,1)S(1)}, u32[]{:S(2)}, u32[]{:S(2)}) %collective-permute-start.14) | collective-permute-done | bytes 393248 | tf_op jit(solution)/shard_map/ppermute | solution.py:26
  331.8 5.4 %convolution_multiply_fusion.2 = f32[768,384]{1,0:T(8,128)} fusion(bf16[768,2048]{0,1:T(8,128)(2,1)} %bitcast.222, bf16[2048,768]{1,0:T(8,128)(2,1)} %all-gather.3.cloned.1.call-done, f32[384]{0:T(512)S(1)} %copy-done.24), kind=kOutput, calls=%fused_computation.47 | convolution fusion | flops 1208254464 | bytes 5899776 | tf_op jit(solution)/shard_map/dot_general | solution.py:145
  337.2 7.3 %convolution_convert_fusion = bf16[768,2048]{1,0:T(8,128)(2,1)} fusion(bf16[384,2048]{0,1:T(8,128)(2,1)} %bitcast.12, bf16[768,2048]{0,1:T(8,128)(2,1)S(1)} %bitcast.223, bf16[2048,768]{1,0:T(8,128)(2,1)} %all-gather.3.cloned.1.call-done, f32[768,384]{1,0:T(8,128)} %convolution_multiply_fusion.2, f32[384]{0:T(512)S(1)} %copy-done.26), kind=kOutput, calls=%fused_computation.39 | convolution fusion | flops 2419556352 | bytes 10618368 | tf_op jit(solution)/shard_map/dot_general | solution.py:148
  346.6 47.0 %all_to_all.48 = bf16[8,768,256]{2,1,0:T(8,128)(2,1)S(1)} all-to-all(bf16[8,768,256]{2,1,0:T(8,128)(2,1)S(1)} %bitcast.215), channel_id=1, replica_groups=mesh['fs'=16,'tp'=8] {'tp'}, dimensions={0} | all-to-all | bytes 6291456 | tf_op jit(solution)/shard_map/all_to_all | solution.py:52
  (219 shorter events, 135.0 us)
Async XLA Ops:
  6.5 65.2 %all-gather.3.cloned.1.call-start = ((), (), s32[]{:S(2)}) async-start(), calls=%async_computation.8 | async-start | bytes 3342336 | tf_op jit(solution)/shard_map/all_gather | solution.py:59
  27.7 7.2 %collective-permute-start.1 = (bf16[768,256]{1,0:T(8,128)(2,1)S(1)}, bf16[768,256]{1,0:T(8,128)(2,1)S(1)}, u32[]{:S(2)}, u32[]{:S(2)}) collective-permute-start(bf16[768,256]{1,0:T(8,128)(2,1)S(1)} %collective-permute-done), channel_id=1, source_target_pairs={{0,1},{1,2},{2,3},{3,4},{4,5},{5,6},{6,7},{7,0},{8,9},{9,10},{10,1... | collective-permute-start | bytes 1179656 | tf_op jit(solution)/shard_map/ppermute | solution.py:26
  30.2 7.5 %collective-permute-start.4 = (bf16[768,256]{1,0:T(8,128)(2,1)S(1)}, bf16[768,256]{1,0:T(8,128)(2,1)S(1)}, u32[]{:S(2)}, u32[]{:S(2)}) collective-permute-start(bf16[768,256]{1,0:T(8,128)(2,1)S(1)} %fusion.54), channel_id=1, source_target_pairs={{1,0},{2,1},{3,2},{4,3},{5,4},{6,5},{7,6},{0,7},{9,8},{10,9},{11,1... | collective-permute-start | bytes 1179656 | tf_op jit(solution)/shard_map/ppermute | solution.py:28
  34.9 7.2 %collective-permute-start.2 = (bf16[768,256]{1,0:T(8,128)(2,1)S(1)}, bf16[768,256]{1,0:T(8,128)(2,1)S(1)}, u32[]{:S(2)}, u32[]{:S(2)}) collective-permute-start(bf16[768,256]{1,0:T(8,128)(2,1)S(1)} %collective-permute-done.1), channel_id=1, source_target_pairs={{0,1},{1,2},{2,3},{3,4},{4,5},{5,6},{6,7},{7,0},{8,9},{9,10},{10,1... | collective-permute-start | bytes 1179656 | tf_op jit(solution)/shard_map/ppermute | solution.py:26
  37.7 18.2 %collective-permute-start.5 = (bf16[768,256]{1,0:T(8,128)(2,1)S(1)}, bf16[768,256]{1,0:T(8,128)(2,1)S(1)}, u32[]{:S(2)}, u32[]{:S(2)}) collective-permute-start(bf16[768,256]{1,0:T(8,128)(2,1)S(1)} %collective-permute-done.4), channel_id=1, source_target_pairs={{1,0},{2,1},{3,2},{4,3},{5,4},{6,5},{7,6},{0,7},{9,8},{10,9},{11,1... | collective-permute-start | bytes 1179656 | tf_op jit(solution)/shard_map/ppermute | solution.py:28
  42.1 17.5 %collective-permute-start.3 = (bf16[768,256]{1,0:T(8,128)(2,1)S(1)}, bf16[768,256]{1,0:T(8,128)(2,1)S(1)}, u32[]{:S(2)}, u32[]{:S(2)}) collective-permute-start(bf16[768,256]{1,0:T(8,128)(2,1)S(1)} %collective-permute-done.2), channel_id=1, source_target_pairs={{0,1},{1,2},{2,3},{3,4},{4,5},{5,6},{6,7},{7,0},{8,9},{9,10},{10,1... | collective-permute-start | bytes 1179656 | tf_op jit(solution)/shard_map/ppermute | solution.py:26
  47.0 30.1 %all-to-all-start.1 = ((bf16[16,384,128]{1,2,0:T(8,128)(2,1)}), bf16[16,384,128]{1,2,0:T(8,128)(2,1)}, u32[]{:S(2)}, u32[]{:S(2)}) async-start(bf16[16,384,128]{1,2,0:T(8,128)(2,1)} %broadcast_in_dim.24), calls=%async_computation.1 | async-start | bytes 3145728 | tf_op jit(solution)/shard_map/all_to_all | solution.py:37
  54.9 147.3 %all-gather.5.cloned.1.call-start = ((), (), s32[]{:S(2)}) async-start(), calls=%async_computation.9 | async-start | bytes 4456448 | tf_op jit(solution)/shard_map/all_gather | solution.py:59
  55.9 9.5 %collective-permute-start.6 = (bf16[768,256]{1,0:T(8,128)(2,1)S(1)}, bf16[768,256]{1,0:T(8,128)(2,1)S(1)}, u32[]{:S(2)}, u32[]{:S(2)}) collective-permute-start(bf16[768,256]{1,0:T(8,128)(2,1)S(1)} %collective-permute-done.5), channel_id=1, source_target_pairs={{1,0},{2,1},{3,2},{4,3},{5,4},{6,5},{7,6},{0,7},{9,8},{10,9},{11,1... | collective-permute-start | bytes 1179656 | tf_op jit(solution)/shard_map/ppermute | solution.py:28
  88.5 48.3 %all-to-all-start.2 = ((bf16[8,768,256]{2,1,0:T(8,128)(2,1)}), bf16[8,768,256]{2,1,0:T(8,128)(2,1)S(1)}, u32[]{:S(2)}, u32[]{:S(2)}) async-start(bf16[8,768,256]{2,1,0:T(8,128)(2,1)} %bitcast.172), calls=%async_computation.2 | async-start | bytes 6291456 | tf_op jit(solution)/shard_map/all_to_all | solution.py:52
  145.8 5.6 %collective-permute-start.7 = (bf16[768,256]{1,0:T(8,128)(2,1)S(1)}, bf16[768,256]{1,0:T(8,128)(2,1)S(1)}, u32[]{:S(2)}, u32[]{:S(2)}) collective-permute-start(bf16[768,256]{1,0:T(8,128)(2,1)S(1)} %fusion.58), channel_id=1, source_target_pairs={{0,1},{1,2},{2,3},{3,4},{4,5},{5,6},{6,7},{7,0},{8,9},{9,10},{10,1... | collective-permute-start | bytes 1179656 | tf_op jit(solution)/shard_map/ppermute | solution.py:26
  151.4 7.2 %collective-permute-start.8 = (bf16[768,256]{1,0:T(8,128)(2,1)S(1)}, bf16[768,256]{1,0:T(8,128)(2,1)S(1)}, u32[]{:S(2)}, u32[]{:S(2)}) collective-permute-start(bf16[768,256]{1,0:T(8,128)(2,1)S(1)} %collective-permute-done.7), channel_id=1, source_target_pairs={{0,1},{1,2},{2,3},{3,4},{4,5},{5,6},{6,7},{7,0},{8,9},{9,10},{10,1... | collective-permute-start | bytes 1179656 | tf_op jit(solution)/shard_map/ppermute | solution.py:26
  153.9 13.8 %collective-permute-start.11 = (bf16[768,256]{1,0:T(8,128)(2,1)S(1)}, bf16[768,256]{1,0:T(8,128)(2,1)S(1)}, u32[]{:S(2)}, u32[]{:S(2)}) collective-permute-start(bf16[768,256]{1,0:T(8,128)(2,1)S(1)} %fusion.58), channel_id=1, source_target_pairs={{1,0},{2,1},{3,2},{4,3},{5,4},{6,5},{7,6},{0,7},{9,8},{10,9},{11,1... | collective-permute-start | bytes 1179656 | tf_op jit(solution)/shard_map/ppermute | solution.py:28
  158.6 11.4 %collective-permute-start.9 = (bf16[768,256]{1,0:T(8,128)(2,1)S(1)}, bf16[768,256]{1,0:T(8,128)(2,1)S(1)}, u32[]{:S(2)}, u32[]{:S(2)}) collective-permute-start(bf16[768,256]{1,0:T(8,128)(2,1)S(1)} %collective-permute-done.8), channel_id=1, source_target_pairs={{0,1},{1,2},{2,3},{3,4},{4,5},{5,6},{6,7},{7,0},{8,9},{9,10},{10,1... | collective-permute-start | bytes 1179656 | tf_op jit(solution)/shard_map/ppermute | solution.py:26
  163.2 73.4 %all-to-all-start.4 = ((bf16[16,256,128]{1,2,0:T(8,128)(2,1)}), bf16[16,256,128]{1,2,0:T(8,128)(2,1)}, u32[]{:S(2)}, u32[]{:S(2)}) async-start(bf16[16,256,128]{1,2,0:T(8,128)(2,1)} %broadcast_in_dim.29), calls=%async_computation.4 | async-start | bytes 2097152 | tf_op jit(solution)/shard_map/all_to_all | solution.py:37
  167.7 15.8 %collective-permute-start.12 = (bf16[768,256]{1,0:T(8,128)(2,1)S(1)}, bf16[768,256]{1,0:T(8,128)(2,1)S(1)}, u32[]{:S(2)}, u32[]{:S(2)}) collective-permute-start(bf16[768,256]{1,0:T(8,128)(2,1)S(1)} %collective-permute-done.11), channel_id=1, source_target_pairs={{1,0},{2,1},{3,2},{4,3},{5,4},{6,5},{7,6},{0,7},{9,8},{10,9},{11,1... | collective-permute-start | bytes 1179656 | tf_op jit(solution)/shard_map/ppermute | solution.py:28
  170.0 16.5 %collective-permute-start.10 = (bf16[768,256]{1,0:T(8,128)(2,1)S(1)}, bf16[768,256]{1,0:T(8,128)(2,1)S(1)}, u32[]{:S(2)}, u32[]{:S(2)}) collective-permute-start(bf16[768,256]{1,0:T(8,128)(2,1)S(1)} %collective-permute-done.9), channel_id=1, source_target_pairs={{0,1},{1,2},{2,3},{3,4},{4,5},{5,6},{6,7},{7,0},{8,9},{9,10},{10,1... | collective-permute-start | bytes 1179656 | tf_op jit(solution)/shard_map/ppermute | solution.py:26
  183.5 8.7 %collective-permute-start.13 = (bf16[768,256]{1,0:T(8,128)(2,1)S(1)}, bf16[768,256]{1,0:T(8,128)(2,1)S(1)}, u32[]{:S(2)}, u32[]{:S(2)}) collective-permute-start(bf16[768,256]{1,0:T(8,128)(2,1)S(1)} %collective-permute-done.12), channel_id=1, source_target_pairs={{1,0},{2,1},{3,2},{4,3},{5,4},{6,5},{7,6},{0,7},{9,8},{10,9},{11,1... | collective-permute-start | bytes 1179656 | tf_op jit(solution)/shard_map/ppermute | solution.py:28
  298.3 7.2 %collective-permute-start.15 = (bf16[768,256]{1,0:T(8,128)(2,1)S(1)}, bf16[768,256]{1,0:T(8,128)(2,1)S(1)}, u32[]{:S(2)}, u32[]{:S(2)}) collective-permute-start(bf16[768,256]{1,0:T(8,128)(2,1)S(1)} %collective-permute-done.14), channel_id=1, source_target_pairs={{0,1},{1,2},{2,3},{3,4},{4,5},{5,6},{6,7},{7,0},{8,9},{9,10},{10,1... | collective-permute-start | bytes 1179656 | tf_op jit(solution)/shard_map/ppermute | solution.py:26
  300.8 7.5 %collective-permute-start.18 = (bf16[768,256]{1,0:T(8,128)(2,1)S(1)}, bf16[768,256]{1,0:T(8,128)(2,1)S(1)}, u32[]{:S(2)}, u32[]{:S(2)}) collective-permute-start(bf16[768,256]{1,0:T(8,128)(2,1)S(1)} %fusion.62), channel_id=1, source_target_pairs={{1,0},{2,1},{3,2},{4,3},{5,4},{6,5},{7,6},{0,7},{9,8},{10,9},{11,1... | collective-permute-start | bytes 1179656 | tf_op jit(solution)/shard_map/ppermute | solution.py:28
  305.5 7.2 %collective-permute-start.16 = (bf16[768,256]{1,0:T(8,128)(2,1)S(1)}, bf16[768,256]{1,0:T(8,128)(2,1)S(1)}, u32[]{:S(2)}, u32[]{:S(2)}) collective-permute-start(bf16[768,256]{1,0:T(8,128)(2,1)S(1)} %collective-permute-done.15), channel_id=1, source_target_pairs={{0,1},{1,2},{2,3},{3,4},{4,5},{5,6},{6,7},{7,0},{8,9},{9,10},{10,1... | collective-permute-start | bytes 1179656 | tf_op jit(solution)/shard_map/ppermute | solution.py:26
  308.3 7.5 %collective-permute-start.19 = (bf16[768,256]{1,0:T(8,128)(2,1)S(1)}, bf16[768,256]{1,0:T(8,128)(2,1)S(1)}, u32[]{:S(2)}, u32[]{:S(2)}) collective-permute-start(bf16[768,256]{1,0:T(8,128)(2,1)S(1)} %collective-permute-done.18), channel_id=1, source_target_pairs={{1,0},{2,1},{3,2},{4,3},{5,4},{6,5},{7,6},{0,7},{9,8},{10,9},{11,1... | collective-permute-start | bytes 1179656 | tf_op jit(solution)/shard_map/ppermute | solution.py:28
  312.7 7.2 %collective-permute-start.17 = (bf16[768,256]{1,0:T(8,128)(2,1)S(1)}, bf16[768,256]{1,0:T(8,128)(2,1)S(1)}, u32[]{:S(2)}, u32[]{:S(2)}) collective-permute-start(bf16[768,256]{1,0:T(8,128)(2,1)S(1)} %collective-permute-done.16), channel_id=1, source_target_pairs={{0,1},{1,2},{2,3},{3,4},{4,5},{5,6},{6,7},{7,0},{8,9},{9,10},{10,1... | collective-permute-start | bytes 1179656 | tf_op jit(solution)/shard_map/ppermute | solution.py:26
  315.8 9.7 %collective-permute-start.20 = (bf16[768,256]{1,0:T(8,128)(2,1)S(1)}, bf16[768,256]{1,0:T(8,128)(2,1)S(1)}, u32[]{:S(2)}, u32[]{:S(2)}) collective-permute-start(bf16[768,256]{1,0:T(8,128)(2,1)S(1)} %collective-permute-done.19), channel_id=1, source_target_pairs={{1,0},{2,1},{3,2},{4,3},{5,4},{6,5},{7,6},{0,7},{9,8},{10,9},{11,1... | collective-permute-start | bytes 1179656 | tf_op jit(solution)/shard_map/ppermute | solution.py:28
  (34 other events, 383.4 us)
Sparse Core Ops, SparseCore 0:
  9.5 51.8 all-gather.2
  63.5 64.2 all-gather.4
